TPU v7x, 32 devices: a whole 2x2x4 slice. The times are simulated.
32 devices in a mesh: grp: 2 (over y), sp: 8 (over z, core), tp: 2 (over x).
Axes of the slice: x: 2, y: 2, z: 4, core: 2. Of those that a mesh axis runs over, the one named last changes fastest.
Arguments:
- tokens: bfloat16 [12288, 2048], P(('grp', 'sp'), 'tp'), parts along dimension 0, may hold values from -4000 to 4000
- gain: float32 [2048], replicated, may hold values from 0.1 to 1.9
- w_query: bfloat16 [2048, 1024], P('sp', 'tp'), may hold values from -1 to 1
- w_key: bfloat16 [2048, 256], P('sp', 'tp'), may hold values from -1 to 1
- w_value: bfloat16 [2048, 256], P('sp', 'tp'), may hold values from -0.125 to 0.125
- w_input: bfloat16 [2048, 1024], P('sp', 'tp'), may hold values from -0.125 to 0.125
- w_bgate: bfloat16 [2048, 1024], P('sp', 'tp'), may hold values from -0.125 to 0.125
- w_cgate: bfloat16 [2048, 1024], P('sp', 'tp'), may hold values from -0.125 to 0.125
- w_attn_out: bfloat16 [1024, 2048], P('sp', 'tp'), may hold values from -2 to 2
- w_conv_out: bfloat16 [1024, 2048], P('sp', 'tp'), may hold values from -0.1875 to 0.1875
- sink_logit: float32 [16], P('tp'), may hold values from 0 to 5
- taps: float32 [3, 1024], P(None, 'tp'), may hold values from -3.5 to 3.5
- conv_bias: float32 [1024], P('tp'), may hold values from -4 to 4
- documents: int32 [12288], P(('grp', 'sp')), parts along dimension 0, may hold values from 0 to 3, never falling along the last dimension, each value on 1 to 3072 neighbouring positions
Outputs:
- mixed: bfloat16 [12288, 2048], P(('grp', 'sp'), 'tp'), parts along dimension 0
There are 2 independent parts, one for each index of `grp`. A program takes and returns all parts, laid end to end along the dimension named above; an argument that names none is the same for every part. Nothing has to cross between parts.
All inputs are finite; a program needn't handle non-finite values.
Results may differ from a plain program's by a relative error of at most 0.013.
The roundings to bfloat16 on the way count: a program that leaves them out, or rounds other values in their place, can miss the bound.
Values may be sent and summed in bfloat16 or wider, within the bound.
A program may use at most 64 MiB of HBM per device.

v0:
```python
import jax
import jax.numpy as jnp
from jax import lax
from jax.sharding import PartitionSpec as P

HEAD_DIM = 64
WINDOW = 128
EPS = 1e-06
THETA = 500000.0


def extended(cells, sides, width):
    for axis, dim in sides:
        count = lax.axis_size(axis)
        ends = count - 1
        head = lax.slice_in_dim(cells, 0, width, axis=dim)
        tail = lax.slice_in_dim(cells, cells.shape[dim] - width, cells.shape[dim], axis=dim)
        cells = jnp.concatenate(
            [
                lax.ppermute(tail, axis, [(i, (i + 1) % count) for i in range(ends)]),
                cells,
                lax.ppermute(head, axis, [((i + 1) % count, i) for i in range(ends)]),
            ],
            axis=dim,
        )
    return cells


def rotate(proj, positions, heads):
    rows = proj.shape[0]
    size = proj.shape[1] // heads
    half = size // 2
    freq = jnp.power(THETA, -(jnp.arange(half, dtype=jnp.float32) * (2.0 / size)))
    angle = positions.astype(jnp.float32)[:, None] * freq[None, :]
    cosine = jnp.cos(angle)[:, None, :]
    sine = jnp.sin(angle)[:, None, :]
    shaped = proj.reshape(rows, heads, size)
    first = shaped[..., :half]
    second = shaped[..., half:]
    turned = jnp.concatenate(
        [first * cosine - second * sine, second * cosine + first * sine], axis=-1
    )
    return turned.reshape(rows, heads * size)


def sink_softmax(scores, allowed, sinks):
    masked = jnp.where(allowed, scores, -jnp.inf)
    top = jnp.maximum(jnp.max(masked, axis=-1, keepdims=True), sinks)
    expo = jnp.exp(masked - top)
    return expo / (jnp.sum(expo, axis=-1, keepdims=True) + jnp.exp(sinks - top))


def local(
    tokens,
    gain,
    w_query,
    w_key,
    w_value,
    w_input,
    w_bgate,
    w_cgate,
    w_attn_out,
    w_conv_out,
    sink_logit,
    taps,
    conv_bias,
    documents,
):
    f32 = jnp.float32
    bf16 = jnp.bfloat16
    rows, part = tokens.shape
    tp_count = lax.axis_size("tp")
    sp_count = lax.axis_size("sp")
    width = part * tp_count
    head_dim = HEAD_DIM
    q_local = w_query.shape[1] // head_dim
    kv_local = w_key.shape[1] // head_dim
    groups = q_local // kv_local
    wq, wk, wv, wu, wb, wc, w_attn, w_conv = (
        lax.all_gather(w_query, "sp", axis=0, tiled=True),
        lax.all_gather(w_key, "sp", axis=0, tiled=True),
        lax.all_gather(w_value, "sp", axis=0, tiled=True),
        lax.all_gather(w_input, "sp", axis=0, tiled=True),
        lax.all_gather(w_bgate, "sp", axis=0, tiled=True),
        lax.all_gather(w_cgate, "sp", axis=0, tiled=True),
        lax.all_gather(w_attn_out, "sp", axis=0, tiled=True),
        lax.all_gather(w_conv_out, "sp", axis=0, tiled=True),
    )
    matrices = (wq, wk, wv, wu, wb, wc)
    piece_f = lax.all_gather(tokens, "tp", axis=1, tiled=True).astype(f32)
    scaled = (piece_f * gain[None, :]).astype(bf16)
    products = tuple((jnp.dot(scaled, mat, preferred_element_type=f32) for mat in matrices))
    folded = products + (jnp.sum(piece_f * piece_f, axis=1),)
    sums = folded[:6]
    squares = folded[6]
    inv = lax.rsqrt(squares / width + EPS)[:, None]
    q_acc, k_acc, v_acc, u_acc, b_acc, c_acc = sums
    positions = lax.axis_index("sp") * rows + jnp.arange(rows, dtype=jnp.int32)
    query = rotate(q_acc * inv, positions, q_local).astype(bf16)
    keys = rotate(k_acc * inv, positions, kv_local).astype(bf16)
    values = (v_acc * inv).astype(bf16)
    carried = (c_acc * inv * (u_acc * inv)).astype(bf16)
    bgate = b_acc * inv
    doc_col = documents.astype(f32).astype(bf16)[:, None]
    paired = jnp.concatenate([keys, values], axis=1)
    pair_ext, doc_ext = (
        extended(paired, (("sp", 0),), WINDOW),
        extended(doc_col, (("sp", 0),), WINDOW),
    )
    carry_ext, doc_near = (extended(carried, (("sp", 0),), 1), extended(doc_col, (("sp", 0),), 1))
    key_width = kv_local * head_dim
    key_ext = pair_ext[:, :key_width].reshape(-1, kv_local, head_dim)
    val_ext = pair_ext[:, key_width:].reshape(-1, kv_local, head_dim)
    key_doc = doc_ext[:, 0].astype(f32)
    own_doc = doc_col[:, 0].astype(f32)
    key_pos = positions[0] - WINDOW + jnp.arange(rows + 2 * WINDOW, dtype=jnp.int32)
    total = sp_count * rows
    sinks = sink_logit.reshape(kv_local, groups, 1, 1)
    block = rows // 2
    outputs = []
    for begin in range(0, rows, block):
        span = block + 2 * WINDOW
        q_block = query[begin : begin + block].reshape(block, kv_local, groups, head_dim)
        k_block = key_ext[begin : begin + span]
        v_block = val_ext[begin : begin + span]
        q_pos = positions[begin : begin + block]
        k_pos = key_pos[begin : begin + span]
        scores = jnp.einsum(
            "qhgd,khd->hgqk", q_block, k_block, preferred_element_type=f32
        ) * head_dim ** (-0.5)
        allowed = jnp.abs(q_pos[:, None] - k_pos[None, :]) <= WINDOW
        allowed = allowed & (
            own_doc[begin : begin + block, None] == key_doc[None, begin : begin + span]
        )
        allowed = allowed & (k_pos >= 0)[None, :] & (k_pos < total)[None, :]
        weight = sink_softmax(scores, allowed, sinks).astype(bf16)
        result = jnp.einsum("hgqk,khd->qhgd", weight, v_block, preferred_element_type=f32)
        outputs.append(result.astype(bf16).reshape(block, q_local * head_dim))
    attended = jnp.concatenate(outputs, axis=0)
    near_doc = doc_near[:, 0].astype(f32)
    conv = jnp.zeros((rows, carried.shape[1]), f32)
    for tap in range(3):
        same = (near_doc[tap : tap + rows] == near_doc[1 : rows + 1])[:, None]
        conv = conv + jnp.where(
            same, carry_ext[tap : tap + rows].astype(f32) * taps[tap][None, :], 0.0
        )
    convolved = (bgate * (conv + conv_bias[None, :])).astype(bf16)
    acc = jnp.dot(
        lax.all_gather(attended, "tp", axis=1, tiled=True), w_attn, preferred_element_type=f32
    )
    mixed = acc + jnp.dot(
        lax.all_gather(convolved, "tp", axis=1, tiled=True), w_conv, preferred_element_type=f32
    )
    return mixed.astype(bf16)


def solution(mesh):
    placed = (
        P(("grp", "sp"), "tp"),
        P(),
        P("sp", "tp"),
        P("sp", "tp"),
        P("sp", "tp"),
        P("sp", "tp"),
        P("sp", "tp"),
        P("sp", "tp"),
        P("sp", "tp"),
        P("sp", "tp"),
        P("tp"),
        P(None, "tp"),
        P("tp"),
        P(("grp", "sp")),
    )
    return jax.shard_map(
        local, mesh=mesh, in_specs=placed, out_specs=P(("grp", "sp"), "tp"), check_vma=False
    )
```

profile of v0, /device:TPU:0, one launch (start us, length us, event | category | flops | bytes accessed | tf_op | source)
XLA Modules:
  0.0 308.4 jit_solution(10480472641820720276)
XLA Ops:
  12.0 3.0 collective-permute-start.1
  16.3 17.1 %all_gather.35 = bf16[2048,128]{1,0:T(8,128)(2,1)S(1)} all-gather(bf16[256,128]{1,0:T(8,128)(2,1)} %param.18), channel_id=1, replica_groups=mesh['grp'=2,'sp'=8,'tp'=2] {'sp'}, dimensions={0}, use_global_device_ids=true | all-gather | bytes 589824 | tf_op jit(solution)/shard_map/all_gather | solution.py:82
  33.4 14.7 %all_gather.34 = bf16[2048,128]{1,0:T(8,128)(2,1)S(1)} all-gather(bf16[256,128]{1,0:T(8,128)(2,1)S(1)} %copy-done.3), channel_id=1, replica_groups=mesh['grp'=2,'sp'=8,'tp'=2] {'sp'}, dimensions={0}, use_global_device_ids=true | all-gather | bytes 589824 | tf_op jit(solution)/shard_map/all_gather | solution.py:81
  49.4 7.1 %all-gather.10.cloned.1.call-done = bf16[768,2048]{1,0:T(8,128)(2,1)} async-done(((bf16[768,1024]{1,0:T(8,128)(2,1)}), bf16[768,2048]{1,0:T(8,128)(2,1)}) %all-gather.10.cloned.1.call-update) | async-done | bytes 3145744 | tf_op jit(solution)/shard_map/all_gather | solution.py:90
  56.5 2.7 fusion.3
  61.9 1.6 collective-permute-start
  63.5 1.5 collective-permute-start.3
  65.7 2.3 collective-permute-done.3
  68.1 19.9 %all-gather.12.cloned.1.call-done = bf16[2048,512]{1,0:T(8,128)(2,1)} async-done(((bf16[256,512]{1,0:T(8,128)(2,1)}), bf16[2048,512]{1,0:T(8,128)(2,1)}) %all-gather.12.cloned.1.call-update) | async-done | bytes 2097168 | tf_op jit(solution)/shard_map/all_gather | solution.py:80
  88.0 4.4 %convolution_multiply_fusion = f32[768,512]{0,1:T(8,128)S(1)} fusion(bf16[2048,512]{1,0:T(8,128)(2,1)} %all-gather.12.cloned.1.call-done, bf16[768,2048]{1,0:T(8,128)(2,1)} %all-gather.10.cloned.1.call-done, f32[2048]{0:T(1024)S(1)} %copy-done.5, f32[768]{0:T(1024)S(1)} %add_rsqrt_fusion), kind=kOutput, calls=%fused_computation.19 | convolution fusion | flops 1615724544 | bytes 6827008 | tf_op jit(solution)/shard_map/dot_general | solution.py:92
  92.7 1.4 fusion.4
  94.2 1.6 fusion
  95.8 1.4 fusion.5
  97.3 1.7 fusion.1
  99.0 2.6 fusion.18
  101.6 2.6 fusion.19
  107.8 3.6 %collective-permute-start.4 = (bf16[1,1]{0,1:T(2,128)(2,1)}, bf16[1,1]{0,1:T(2,128)(2,1)}, u32[]{:S(2)}, u32[]{:S(2)}) collective-permute-start(bf16[1,1]{0,1:T(2,128)(2,1)} %bitcast.26), channel_id=1, source_target_pairs={{0,2},{2,4},{4,6},{6,8},{8,10},{10,12},{12,14},{1,3},{3,5},{5,7},{... | collective-permute-start | bytes 14 | tf_op jit(solution)/shard_map/ppermute | solution.py:20
  111.8 1.4 maximum_convert_fusion.1
  113.2 5.0 %all-gather.20.cloned.1.call-done = bf16[2048,512]{1,0:T(8,128)(2,1)} async-done(((bf16[256,512]{1,0:T(8,128)(2,1)}), bf16[2048,512]{1,0:T(8,128)(2,1)}) %all-gather.20.cloned.1.call-update) | async-done | bytes 2097168 | tf_op jit(solution)/shard_map/all_gather | solution.py:85
  118.2 5.5 %fusion.9 = f32[768,512]{0,1:T(8,128)} fusion(bf16[2048,512]{1,0:T(8,128)(2,1)} %all-gather.20.cloned.1.call-done, bf16[768,2048]{1,0:T(8,128)(2,1)} %all-gather.10.cloned.1.call-done, f32[2048]{0:T(1024)S(1)} %copy-done.5), kind=kOutput, calls=%fused_computation.20 | convolution fusion | flops 1615331328 | bytes 6823936 | tf_op jit(solution)/shard_map/dot_general | solution.py:92
  123.7 24.5 %all-gather.22.cloned.1.call-done = bf16[2048,512]{1,0:T(8,128)(2,1)} async-done(((bf16[256,512]{1,0:T(8,128)(2,1)}), bf16[2048,512]{1,0:T(8,128)(2,1)}) %all-gather.22.cloned.1.call-update) | async-done | bytes 2097168 | tf_op jit(solution)/shard_map/all_gather | solution.py:83
  148.2 3.9 %multiply_convert_fusion.1 = bf16[768,512]{0,1:T(8,128)(2,1)S(1)} fusion(f32[768,512]{0,1:T(8,128)} %fusion.9, bf16[2048,512]{1,0:T(8,128)(2,1)} %all-gather.22.cloned.1.call-done, bf16[768,2048]{1,0:T(8,128)(2,1)S(1)} %copy-done.1, f32[2048]{0:T(1024)S(1)} %copy-done.5, f32[768]{0:T(1024)S(1)} %add_rsqrt_fusion), kind=kOutput, calls=%fused_computation.18 | convolution fusion | flops 1616904192 | bytes 7613440 | tf_op jit(solution)/shard_map/dot_general | solution.py:92
  152.3 1.3 collective-permute-start.7
  153.6 3.7 %collective-permute-start.6 = (bf16[1,512]{0,1:T(8,128)(2,1)S(1)}, bf16[1,512]{0,1:T(8,128)(2,1)}, u32[]{:S(2)}, u32[]{:S(2)}) collective-permute-start(bf16[1,512]{0,1:T(8,128)(2,1)S(1)} %get-tuple-element.12), channel_id=1, source_target_pairs={{0,2},{2,4},{4,6},{6,8},{8,10},{10,12},{12,14},{1,3},{3,5},{5,7},{... | collective-permute-start | bytes 3080 | tf_op jit(solution)/shard_map/ppermute | solution.py:20
  157.4 20.9 %all-gather.18.cloned.1.call-done = bf16[2048,512]{1,0:T(8,128)(2,1)} async-done(((bf16[256,512]{1,0:T(8,128)(2,1)}), bf16[2048,512]{1,0:T(8,128)(2,1)}) %all-gather.18.cloned.1.call-update) | async-done | bytes 2097168 | tf_op jit(solution)/shard_map/all_gather | solution.py:84
  178.3 5.7 %multiply_convert_fusion = bf16[768,512]{0,1:T(8,128)(2,1)} fusion(bf16[768,512]{0,1:T(8,128)(2,1)} %copy-done.2, bf16[1,512]{0,1:T(8,128)(2,1)} %collective-permute-done.7, bf16[1,512]{0,1:T(8,128)(2,1)} %collective-permute-done.6, f32[512]{0:T(512)S(1)} %copy-done.6, f32[512]{0:T(512)S(1)} %bitcast.92, f32[512]{0:T(512)S(1)} %bitcast.93, ...), kind=kOutput, calls=%fused_computation.17 | convolution fusion | flops 1623588864 | bytes 6839552 | tf_op jit(solution)/shard_map/dot_general | solution.py:92
  184.0 25.7 %all-gather.16.cloned.1.call-done = bf16[1024,1024]{1,0:T(8,128)(2,1)} async-done(((bf16[128,1024]{1,0:T(8,128)(2,1)}), bf16[1024,1024]{1,0:T(8,128)(2,1)}) %all-gather.16.cloned.1.call-update) | async-done | bytes 2097168 | tf_op jit(solution)/shard_map/all_gather | solution.py:86
  209.7 28.1 %all-gather.14.cloned.1.call-done = bf16[768,1024]{0,1:T(8,128)(2,1)} async-done(((bf16[768,512]{0,1:T(8,128)(2,1)}), bf16[768,1024]{0,1:T(8,128)(2,1)}) %all-gather.14.cloned.1.call-update) | async-done | bytes 1572880 | tf_op jit(solution)/shard_map/all_gather | solution.py:149
  237.8 3.9 %fusion.47 = f32[768,1024]{1,0:T(8,128)S(1)} fusion(bf16[768,1024]{0,1:T(8,128)(2,1)} %all-gather.14.cloned.1.call-done, bf16[1024,1024]{1,0:T(8,128)(2,1)} %all-gather.16.cloned.1.call-done), kind=kOutput, calls=%fused_computation.92 | convolution fusion | flops 1610612736 | bytes 6815744 | tf_op jit(solution)/shard_map/dot_general | solution.py:148
  241.7 26.9 %all-gather.26.cloned.1.call-done = bf16[1024,1024]{1,0:T(8,128)(2,1)} async-done(((bf16[128,1024]{1,0:T(8,128)(2,1)}), bf16[1024,1024]{1,0:T(8,128)(2,1)}) %all-gather.26.cloned.1.call-update) | async-done | bytes 2097168 | tf_op jit(solution)/shard_map/all_gather | solution.py:87
  268.6 28.2 %all-gather.24.cloned.1.call-done = bf16[768,1024]{0,1:T(8,128)(2,1)} async-done(((bf16[768,512]{0,1:T(8,128)(2,1)}), bf16[768,1024]{0,1:T(8,128)(2,1)}) %all-gather.24.cloned.1.call-update) | async-done | bytes 1572880 | tf_op jit(solution)/shard_map/all_gather | solution.py:152
  296.8 5.0 %add_convert_fusion = bf16[768,1024]{1,0:T(8,128)(2,1)} fusion(f32[768,1024]{1,0:T(8,128)S(1)} %fusion.47, bf16[768,1024]{0,1:T(8,128)(2,1)} %all-gather.24.cloned.1.call-done, bf16[1024,1024]{1,0:T(8,128)(2,1)} %all-gather.26.cloned.1.call-done), kind=kOutput, calls=%fused_computation.16 | convolution fusion | flops 1612185600 | bytes 8388608 | tf_op jit(solution)/shard_map/dot_general | solution.py:151
  (77 shorter events, 15.4 us)
Async XLA Ops:
  6.5 26.9 %copy-start.3 = (bf16[256,128]{1,0:T(8,128)(2,1)S(1)}, bf16[256,128]{1,0:T(8,128)(2,1)}, u32[]{:S(2)}) copy-start(bf16[256,128]{1,0:T(8,128)(2,1)} %param.17) | copy-start | bytes 196612
  6.5 42.0 %copy-start.7 = (f32[8]{0:T(128)S(1)}, f32[8]{0:T(128)}, u32[]{:S(2)}) copy-start(f32[8]{0:T(128)} %param.24) | copy-start | bytes 100
  6.5 50.0 %all-gather.10.cloned.1.call-start = ((), (), s32[]{:S(2)}) async-start(), calls=%async_computation | async-start | bytes 4718592 | tf_op jit(solution)/shard_map/all_gather | solution.py:90
  7.3 52.0 %copy-start.5 = (f32[2048]{0:T(1024)S(1)}, f32[2048]{0:T(1024)}, u32[]{:S(2)}) copy-start(f32[2048]{0:T(1024)} %param.15) | copy-start | bytes 24580
  7.3 80.8 %all-gather.12.cloned.1.call-start = ((), (), s32[]{:S(2)}) async-start(), calls=%async_computation.1 | async-start | bytes 2359296 | tf_op jit(solution)/shard_map/all_gather | solution.py:80
  8.0 110.2 %all-gather.20.cloned.1.call-start = ((), (), s32[]{:S(2)}) async-start(), calls=%async_computation.5 | async-start | bytes 2359296 | tf_op jit(solution)/shard_map/all_gather | solution.py:85
  8.8 139.5 %all-gather.22.cloned.1.call-start = ((), (), s32[]{:S(2)}) async-start(), calls=%async_computation.6 | async-start | bytes 2359296 | tf_op jit(solution)/shard_map/all_gather | solution.py:83
  9.3 168.9 %all-gather.18.cloned.1.call-start = ((), (), s32[]{:S(2)}) async-start(), calls=%async_computation.4 | async-start | bytes 2359296 | tf_op jit(solution)/shard_map/all_gather | solution.py:84
  9.9 199.8 %all-gather.16.cloned.1.call-start = ((), (), s32[]{:S(2)}) async-start(), calls=%async_computation.3 | async-start | bytes 2359296 | tf_op jit(solution)/shard_map/all_gather | solution.py:86
  10.7 38.0 %collective-permute-start.2 = (bf16[128,1]{0,1:T(2,128)(2,1)S(1)}, bf16[128,1]{0,1:T(2,128)(2,1)S(1)}, u32[]{:S(2)}, u32[]{:S(2)}) collective-permute-start(bf16[128,1]{0,1:T(2,128)(2,1)S(1)} %get-tuple-element.44), channel_id=1, source_target_pairs={{2,0},{4,2},{6,4},{8,6},{10,8},{12,10},{14,12},{3,1},{5,3},{7,5},{... | collective-permute-start | bytes 776 | tf_op jit(solution)/shard_map/ppermute | solution.py:22
  12.0 36.7 %collective-permute-start.1 = (bf16[128,1]{0,1:T(2,128)(2,1)S(1)}, bf16[128,1]{0,1:T(2,128)(2,1)S(1)}, u32[]{:S(2)}, u32[]{:S(2)}) collective-permute-start(bf16[128,1]{0,1:T(2,128)(2,1)S(1)} %get-tuple-element.43), channel_id=1, source_target_pairs={{0,2},{2,4},{4,6},{6,8},{8,10},{10,12},{12,14},{1,3},{3,5},{5,7},{... | collective-permute-start | bytes 776 | tf_op jit(solution)/shard_map/ppermute | solution.py:20
  15.0 222.8 %all-gather.14.cloned.1.call-start = ((), (), s32[]{:S(2)}) async-start(), calls=%async_computation.2 | async-start | bytes 2359296 | tf_op jit(solution)/shard_map/all_gather | solution.py:149
  56.5 2.8 copy-start
  61.9 3.8 %collective-permute-start = (bf16[128,256]{0,1:T(8,128)(2,1)S(1)}, bf16[128,256]{0,1:T(8,128)(2,1)S(1)}, u32[]{:S(2)}, u32[]{:S(2)}) collective-permute-start(bf16[128,256]{0,1:T(8,128)(2,1)S(1)} %get-tuple-element.24), channel_id=1, source_target_pairs={{0,2},{2,4},{4,6},{6,8},{8,10},{10,12},{12,14},{1,3},{3,5},{5,7},{... | collective-permute-start | bytes 196616 | tf_op jit(solution)/shard_map/ppermute | solution.py:20
  63.5 4.6 %collective-permute-start.3 = (bf16[128,256]{0,1:T(8,128)(2,1)S(1)}, bf16[128,256]{0,1:T(8,128)(2,1)S(1)}, u32[]{:S(2)}, u32[]{:S(2)}) collective-permute-start(bf16[128,256]{0,1:T(8,128)(2,1)S(1)} %get-tuple-element.25), channel_id=1, source_target_pairs={{2,0},{4,2},{6,4},{8,6},{10,8},{12,10},{14,12},{3,1},{5,3},{7,5},{... | collective-permute-start | bytes 196616 | tf_op jit(solution)/shard_map/ppermute | solution.py:22
  101.6 9.9 %copy-start.4 = (f32[3,512]{1,0:T(4,128)S(1)}, f32[3,512]{1,0:T(4,128)}, u32[]{:S(2)}) copy-start(f32[3,512]{1,0:T(4,128)} %param.25) | copy-start | bytes 18436
  105.1 163.5 %all-gather.26.cloned.1.call-start = ((), (), s32[]{:S(2)}) async-start(), calls=%async_computation.8 | async-start | bytes 2359296 | tf_op jit(solution)/shard_map/all_gather | solution.py:87
  105.9 190.9 %all-gather.24.cloned.1.call-start = ((), (), s32[]{:S(2)}) async-start(), calls=%async_computation.7 | async-start | bytes 2359296 | tf_op jit(solution)/shard_map/all_gather | solution.py:152
  106.5 4.9 %collective-permute-start.5 = (bf16[1,1]{0,1:T(2,128)(2,1)}, bf16[1,1]{0,1:T(2,128)(2,1)}, u32[]{:S(2)}, u32[]{:S(2)}) collective-permute-start(bf16[1,1]{0,1:T(2,128)(2,1)} %bitcast.27), channel_id=1, source_target_pairs={{2,0},{4,2},{6,4},{8,6},{10,8},{12,10},{14,12},{3,1},{5,3},{7,5},{... | collective-permute-start | bytes 14 | tf_op jit(solution)/shard_map/ppermute | solution.py:22
  107.8 4.0 %collective-permute-start.4 = (bf16[1,1]{0,1:T(2,128)(2,1)}, bf16[1,1]{0,1:T(2,128)(2,1)}, u32[]{:S(2)}, u32[]{:S(2)}) collective-permute-start(bf16[1,1]{0,1:T(2,128)(2,1)} %bitcast.26), channel_id=1, source_target_pairs={{0,2},{2,4},{4,6},{6,8},{8,10},{10,12},{12,14},{1,3},{3,5},{5,7},{... | collective-permute-start | bytes 14 | tf_op jit(solution)/shard_map/ppermute | solution.py:20
  113.2 35.0 %copy-start.1 = (bf16[768,2048]{1,0:T(8,128)(2,1)S(1)}, bf16[768,2048]{1,0:T(8,128)(2,1)}, u32[]{:S(2)}) copy-start(bf16[768,2048]{1,0:T(8,128)(2,1)} %all-gather.10.cloned.1.call-done) | copy-start | bytes 9437188
  123.7 54.5 %copy-start.6 = (f32[512]{0:T(512)S(1)}, f32[512]{0:T(512)}, u32[]{:S(2)}) copy-start(f32[512]{0:T(512)} %param.26) | copy-start | bytes 6148
  152.1 5.1 %copy-start.2 = (bf16[768,512]{0,1:T(8,128)(2,1)}, bf16[768,512]{0,1:T(8,128)(2,1)S(1)}, u32[]{:S(2)}) copy-start(bf16[768,512]{0,1:T(8,128)(2,1)S(1)} %multiply_convert_fusion.1) | copy-start | bytes 2359300
  152.3 26.0 %collective-permute-start.7 = (bf16[1,512]{0,1:T(8,128)(2,1)S(1)}, bf16[1,512]{0,1:T(8,128)(2,1)}, u32[]{:S(2)}, u32[]{:S(2)}) collective-permute-start(bf16[1,512]{0,1:T(8,128)(2,1)S(1)} %get-tuple-element.13), channel_id=1, source_target_pairs={{2,0},{4,2},{6,4},{8,6},{10,8},{12,10},{14,12},{3,1},{5,3},{7,5},{... | collective-permute-start | bytes 3080 | tf_op jit(solution)/shard_map/ppermute | solution.py:22
  153.6 24.7 %collective-permute-start.6 = (bf16[1,512]{0,1:T(8,128)(2,1)S(1)}, bf16[1,512]{0,1:T(8,128)(2,1)}, u32[]{:S(2)}, u32[]{:S(2)}) collective-permute-start(bf16[1,512]{0,1:T(8,128)(2,1)S(1)} %get-tuple-element.12), channel_id=1, source_target_pairs={{0,2},{2,4},{4,6},{6,8},{8,10},{10,12},{12,14},{1,3},{3,5},{5,7},{... | collective-permute-start | bytes 3080 | tf_op jit(solution)/shard_map/ppermute | solution.py:20
Sparse Core Ops, SparseCore 0:
  8.9 47.6 all-gather.9
  58.1 29.8 all-gather.11
  89.6 28.5 all-gather.19
  119.7 28.5 all-gather.21
  149.7 28.5 all-gather.17
  179.7 29.9 all-gather.15
  211.2 26.5 all-gather.13
  239.4 29.1 all-gather.25
  270.2 26.5 all-gather.23
where the time goes:
time: 309 us; the launch traced here: 308 us
  waiting for transfers between devices  193 us (62%)
  matrix products  38.7 us (13%)
  blocking collectives  31.8 us (10%)
  starting transfers between devices  17.6 us (6%)
  between operations  14.2 us (5%)
  other arithmetic  11.9 us (4%)
    all_gather x1, waiting for transfers between devices, local(): lax.all_gather(convolved, 'tp', axis=1, tiled=True)  28.2 us
    all_gather x1, waiting for transfers between devices, local(): lax.all_gather(attended, 'tp', axis=1, tiled=True)  28.1 us
    all_gather x1, waiting for transfers between devices, local(): lax.all_gather(w_conv_out, 'sp', axis=0, tiled=True)  26.9 us
    all_gather x1, waiting for transfers between devices, local(): lax.all_gather(w_attn_out, 'sp', axis=0, tiled=True)  25.7 us
    all_gather x1, waiting for transfers between devices, local(): lax.all_gather(w_input, 'sp', axis=0, tiled=True)  24.5 us
    dot_general x6, matrix products, local(): jnp.dot(scaled, mat, preferred_element_type=f32)  21.9 us
    all_gather x1, waiting for transfers between devices, local(): lax.all_gather(w_bgate, 'sp', axis=0, tiled=True)  20.9 us
    all_gather x1, waiting for transfers between devices, local(): lax.all_gather(w_query, 'sp', axis=0, tiled=True)  19.9 us
  transfers between devices with their start and end apart: 17, of which 11 were waited for; matrix products, arithmetic and copies ran while one was open for 15% of the time, Pallas kernels for 0%

commit v1 on v0

--- a/solution.py
+++ b/solution.py
@@ -7,6 +7,11 @@
 WINDOW = 128
 EPS = 1e-06
 THETA = 500000.0
+
+
+def all_by_exchange(x, name, dim):
+    stack = jnp.stack([x] * lax.axis_size(name))
+    return jnp.concatenate(lax.all_to_all(stack, name, 0, 0), axis=dim)
 
 
 def extended(cells, sides, width):
@@ -80,7 +85,7 @@
         lax.all_gather(w_query, "sp", axis=0, tiled=True),
         lax.all_gather(w_key, "sp", axis=0, tiled=True),
         lax.all_gather(w_value, "sp", axis=0, tiled=True),
-        lax.all_gather(w_input, "sp", axis=0, tiled=True),
+        all_by_exchange(w_input, "sp", 0),
         lax.all_gather(w_bgate, "sp", axis=0, tiled=True),
         lax.all_gather(w_cgate, "sp", axis=0, tiled=True),
         lax.all_gather(w_attn_out, "sp", axis=0, tiled=True),

time: 309 us -> 287 us (0.929)
  waiting for transfers between devices: 193 us -> 102 us
  blocking collectives: 31.8 us -> 87.5 us
  starting transfers between devices: 17.6 us -> 28.1 us
    all_gather x1, blocking collectives: 17.1 us -> 69.9 us  [local(): lax.all_gather(w_value, 'sp', axis=0, tiled=True)]
    all_gather x1 -> x0, waiting for transfers between devices: 24.5 us -> none  [local(): lax.all_gather(w_input, 'sp', axis=0, tiled=True)]
    all_gather x1, waiting for transfers between devices: 20.9 us -> 0.02 us  [local(): lax.all_gather(w_bgate, 'sp', axis=0, tiled=True)]
    all_gather x1, waiting for transfers between devices: 19.9 us -> 0.02 us  [local(): lax.all_gather(w_query, 'sp', axis=0, tiled=True)]
    all_gather x1, waiting for transfers between devices: 25.7 us -> 12.2 us  [local(): lax.all_gather(w_attn_out, 'sp', axis=0, tiled=True)]
    all_gather x1, waiting for transfers between devices: 7.12 us -> 0.02 us  [local(): piece_f = lax.all_gather(tokens, 'tp', axis=1, tiled=True).astype(f32)]
    all_to_all x0 -> x1, starting transfers between devices: none -> 6.49 us  [all_by_exchange(): return jnp.concatenate(lax.all_to_all(stack, name, 0, 0), axis=dim)]
    all_gather x1, waiting for transfers between devices: 4.96 us -> 0.01 us  [local(): lax.all_gather(w_cgate, 'sp', axis=0, tiled=True)]
  transfers between devices with their start and end apart: 17 -> 17, of which waited for: 11 -> 7; matrix products, arithmetic and copies ran while one was open for 15% -> 17% of each run, Pallas kernels for 0% -> 0%
where the time goes in v1:
time: 287 us; the launch traced here: 286 us
  waiting for transfers between devices  102 us (36%)
  blocking collectives  87.5 us (30%)
  matrix products  38.8 us (14%)
  starting transfers between devices  28.1 us (10%)
  between operations  14.5 us (5%)
  other arithmetic  11.7 us (4%)
  local copies, waits for them, and re-layouts  3.97 us (1%)
    all_gather x1, blocking collectives, local(): lax.all_gather(w_value, 'sp', axis=0, tiled=True)  69.9 us
    all_gather x1, waiting for transfers between devices, local(): lax.all_gather(convolved, 'tp', axis=1, tiled=True)  28.1 us
    all_gather x1, waiting for transfers between devices, local(): lax.all_gather(attended, 'tp', axis=1, tiled=True)  28 us
    all_gather x1, waiting for transfers between devices, local(): lax.all_gather(w_conv_out, 'sp', axis=0, tiled=True)  26.9 us
    dot_general x6, matrix products, local(): jnp.dot(scaled, mat, preferred_element_type=f32)  22.1 us
    all_gather x1, blocking collectives, local(): lax.all_gather(w_key, 'sp', axis=0, tiled=True)  17.6 us
    ppermute x4, starting transfers between devices, extended(): lax.ppermute(tail, axis, [(i, (i + 1) % count) for i in range(ends)])  16 us
    all_gather x1, waiting for transfers between devices, local(): lax.all_gather(w_attn_out, 'sp', axis=0, tiled=True)  12.2 us
  transfers between devices with their start and end apart: 17, of which 7 were waited for; matrix products, arithmetic and copies ran while one was open for 17% of the time, Pallas kernels for 0%

profile of v1, /device:TPU:0, one launch (start us, length us, event | category | flops | bytes accessed | tf_op | source)
XLA Modules:
  0.0 286.5 jit_solution(15820729081790867719)
XLA Ops:
  10.0 1.3 collective-permute-start.2
  11.3 3.2 %collective-permute-start.1 = (bf16[128,1]{0,1:T(2,128)(2,1)S(1)}, bf16[128,1]{0,1:T(2,128)(2,1)S(1)}, u32[]{:S(2)}, u32[]{:S(2)}) collective-permute-start(bf16[128,1]{0,1:T(2,128)(2,1)S(1)} %get-tuple-element.43), channel_id=1, source_target_pairs={{0,2},{2,4},{4,6},{6,8},{8,10},{10,12},{12,14},{1,3},{3,5},{5,7},{... | collective-permute-start | bytes 776 | tf_op jit(solution)/shard_map/ppermute | solution.py:25
  14.5 2.5 stack.2
  16.9 6.5 %all-to-all-start = ((bf16[8,256,512]{2,1,0:T(8,128)(2,1)}), bf16[8,256,512]{2,1,0:T(8,128)(2,1)}, u32[]{:S(2)}, u32[]{:S(2)}) async-start(bf16[8,256,512]{2,1,0:T(8,128)(2,1)} %stack.2), calls=%async_computation | async-start | bytes 4194304 | tf_op jit(solution)/shard_map/all_to_all | solution.py:14
  25.3 69.9 %all_gather.32 = bf16[2048,128]{1,0:T(8,128)(2,1)S(1)} all-gather(bf16[256,128]{1,0:T(8,128)(2,1)S(1)} %copy-done.3), channel_id=1, replica_groups=mesh['grp'=2,'sp'=8,'tp'=2] {'sp'}, dimensions={0}, use_global_device_ids=true | all-gather | bytes 589824 | tf_op jit(solution)/shard_map/all_gather | solution.py:87
  95.3 17.6 %all_gather.31 = bf16[2048,128]{1,0:T(8,128)(2,1)S(1)} all-gather(bf16[256,128]{1,0:T(8,128)(2,1)S(1)} %copy-done.4), channel_id=1, replica_groups=mesh['grp'=2,'sp'=8,'tp'=2] {'sp'}, dimensions={0}, use_global_device_ids=true | all-gather | bytes 589824 | tf_op jit(solution)/shard_map/all_gather | solution.py:86
  114.2 2.7 fusion.3
  117.1 1.2 fusion.20
  119.6 2.3 collective-permute-start
  121.9 1.5 collective-permute-start.3
  124.1 1.7 collective-permute-done.3
  125.9 4.4 %convolution_multiply_fusion = f32[768,512]{0,1:T(8,128)S(1)} fusion(bf16[2048,512]{1,0:T(8,128)(2,1)} %all-gather.11.cloned.1.call-done, bf16[768,2048]{1,0:T(8,128)(2,1)} %all-gather.9.cloned.1.call-done, f32[2048]{0:T(1024)S(1)} %copy-done.6, f32[768]{0:T(1024)S(1)} %add_rsqrt_fusion), kind=kOutput, calls=%fused_computation.19 | convolution fusion | flops 1615724544 | bytes 6827008 | tf_op jit(solution)/shard_map/dot_general | solution.py:97
  130.7 1.4 fusion.4
  132.1 1.6 fusion
  133.7 1.3 fusion.5
  135.2 1.7 fusion.1
  136.9 2.6 fusion.18
  139.5 2.6 fusion.19
  144.4 1.3 collective-permute-start.5
  145.7 6.0 %collective-permute-start.4 = (bf16[1,1]{0,1:T(2,128)(2,1)}, bf16[1,1]{0,1:T(2,128)(2,1)}, u32[]{:S(2)}, u32[]{:S(2)}) collective-permute-start(bf16[1,1]{0,1:T(2,128)(2,1)} %bitcast.26), channel_id=1, source_target_pairs={{0,2},{2,4},{4,6},{6,8},{8,10},{10,12},{12,14},{1,3},{3,5},{5,7},{... | collective-permute-start | bytes 14 | tf_op jit(solution)/shard_map/ppermute | solution.py:25
  152.3 1.3 maximum_convert_fusion.1
  153.6 5.7 %fusion.9 = f32[768,512]{0,1:T(8,128)} fusion(bf16[2048,512]{1,0:T(8,128)(2,1)} %all-gather.19.cloned.1.call-done, bf16[768,2048]{1,0:T(8,128)(2,1)} %all-gather.9.cloned.1.call-done, f32[2048]{0:T(1024)S(1)} %copy-done.6), kind=kOutput, calls=%fused_computation.20 | convolution fusion | flops 1615331328 | bytes 6823936 | tf_op jit(solution)/shard_map/dot_general | solution.py:97
  159.3 3.9 %multiply_convert_fusion.1 = bf16[768,512]{0,1:T(8,128)(2,1)S(1)} fusion(f32[768,512]{0,1:T(8,128)} %fusion.9, bf16[2048,512]{1,0:T(8,128)(2,1)} %bitcast.28, bf16[768,2048]{1,0:T(8,128)(2,1)S(1)} %copy-done.1, f32[2048]{0:T(1024)S(1)} %copy-done.6, f32[768]{0:T(1024)S(1)} %add_rsqrt_fusion), kind=kOutput, calls=%fused_computation.18 | convolution fusion | flops 1616904192 | bytes 7613440 | tf_op jit(solution)/shard_map/dot_general | solution.py:97
  163.3 1.3 collective-permute-start.7
  164.6 4.7 %collective-permute-start.6 = (bf16[1,512]{0,1:T(8,128)(2,1)S(1)}, bf16[1,512]{0,1:T(8,128)(2,1)}, u32[]{:S(2)}, u32[]{:S(2)}) collective-permute-start(bf16[1,512]{0,1:T(8,128)(2,1)S(1)} %get-tuple-element.12), channel_id=1, source_target_pairs={{0,2},{2,4},{4,6},{6,8},{8,10},{10,12},{12,14},{1,3},{3,5},{5,7},{... | collective-permute-start | bytes 3080 | tf_op jit(solution)/shard_map/ppermute | solution.py:25
  169.8 5.7 %multiply_convert_fusion = bf16[768,512]{0,1:T(8,128)(2,1)} fusion(bf16[768,512]{0,1:T(8,128)(2,1)} %copy-done.2, bf16[1,512]{0,1:T(8,128)(2,1)} %collective-permute-done.7, bf16[1,512]{0,1:T(8,128)(2,1)} %collective-permute-done.6, f32[512]{0:T(512)S(1)} %copy-done.7, f32[512]{0:T(512)S(1)} %bitcast.93, f32[512]{0:T(512)S(1)} %bitcast.94, ...), kind=kOutput, calls=%fused_computation.17 | convolution fusion | flops 1623588864 | bytes 6839552 | tf_op jit(solution)/shard_map/dot_general | solution.py:97
  175.5 12.2 %all-gather.15.cloned.1.call-done = bf16[1024,1024]{1,0:T(8,128)(2,1)} async-done(((bf16[128,1024]{1,0:T(8,128)(2,1)}), bf16[1024,1024]{1,0:T(8,128)(2,1)}) %all-gather.15.cloned.1.call-update) | async-done | bytes 2097168 | tf_op jit(solution)/shard_map/all_gather | solution.py:91
  187.6 28.0 %all-gather.13.cloned.1.call-done = bf16[768,1024]{0,1:T(8,128)(2,1)} async-done(((bf16[768,512]{0,1:T(8,128)(2,1)}), bf16[768,1024]{0,1:T(8,128)(2,1)}) %all-gather.13.cloned.1.call-update) | async-done | bytes 1572880 | tf_op jit(solution)/shard_map/all_gather | solution.py:154
  215.6 3.9 %fusion.47 = f32[768,1024]{1,0:T(8,128)S(1)} fusion(bf16[768,1024]{0,1:T(8,128)(2,1)} %all-gather.13.cloned.1.call-done, bf16[1024,1024]{1,0:T(8,128)(2,1)} %all-gather.15.cloned.1.call-done), kind=kOutput, calls=%fused_computation.92 | convolution fusion | flops 1610612736 | bytes 6815744 | tf_op jit(solution)/shard_map/dot_general | solution.py:153
  219.5 26.9 %all-gather.23.cloned.1.call-done = bf16[1024,1024]{1,0:T(8,128)(2,1)} async-done(((bf16[128,1024]{1,0:T(8,128)(2,1)}), bf16[1024,1024]{1,0:T(8,128)(2,1)}) %all-gather.23.cloned.1.call-update) | async-done | bytes 2097168 | tf_op jit(solution)/shard_map/all_gather | solution.py:92
  246.4 28.1 %all-gather.21.cloned.1.call-done = bf16[768,1024]{0,1:T(8,128)(2,1)} async-done(((bf16[768,512]{0,1:T(8,128)(2,1)}), bf16[768,1024]{0,1:T(8,128)(2,1)}) %all-gather.21.cloned.1.call-update) | async-done | bytes 1572880 | tf_op jit(solution)/shard_map/all_gather | solution.py:157
  274.6 5.0 %add_convert_fusion = bf16[768,1024]{1,0:T(8,128)(2,1)} fusion(f32[768,1024]{1,0:T(8,128)S(1)} %fusion.47, bf16[768,1024]{0,1:T(8,128)(2,1)} %all-gather.21.cloned.1.call-done, bf16[1024,1024]{1,0:T(8,128)(2,1)} %all-gather.23.cloned.1.call-done), kind=kOutput, calls=%fused_computation.16 | convolution fusion | flops 1612185600 | bytes 8388608 | tf_op jit(solution)/shard_map/dot_general | solution.py:156
  (79 shorter events, 12.3 us)
Async XLA Ops:
  6.5 107.6 %all-gather.9.cloned.1.call-start = ((), (), s32[]{:S(2)}) async-start(), calls=%async_computation.1 | async-start | bytes 4718592 | tf_op jit(solution)/shard_map/all_gather | solution.py:95
  7.3 118.7 %all-gather.11.cloned.1.call-start = ((), (), s32[]{:S(2)}) async-start(), calls=%async_computation.2 | async-start | bytes 2359296 | tf_op jit(solution)/shard_map/all_gather | solution.py:85
  8.0 145.6 %all-gather.19.cloned.1.call-start = ((), (), s32[]{:S(2)}) async-start(), calls=%async_computation.6 | async-start | bytes 2359296 | tf_op jit(solution)/shard_map/all_gather | solution.py:90
  8.7 160.7 %all-gather.17.cloned.1.call-start = ((), (), s32[]{:S(2)}) async-start(), calls=%async_computation.5 | async-start | bytes 2359296 | tf_op jit(solution)/shard_map/all_gather | solution.py:89
  10.0 103.4 %collective-permute-start.2 = (bf16[128,1]{0,1:T(2,128)(2,1)S(1)}, bf16[128,1]{0,1:T(2,128)(2,1)S(1)}, u32[]{:S(2)}, u32[]{:S(2)}) collective-permute-start(bf16[128,1]{0,1:T(2,128)(2,1)S(1)} %get-tuple-element.44), channel_id=1, source_target_pairs={{2,0},{4,2},{6,4},{8,6},{10,8},{12,10},{14,12},{3,1},{5,3},{7,5},{... | collective-permute-start | bytes 776 | tf_op jit(solution)/shard_map/ppermute | solution.py:27
  11.3 14.0 %copy-start.3 = (bf16[256,128]{1,0:T(8,128)(2,1)S(1)}, bf16[256,128]{1,0:T(8,128)(2,1)}, u32[]{:S(2)}) copy-start(bf16[256,128]{1,0:T(8,128)(2,1)} %param.18) | copy-start | bytes 196612
  11.3 102.1 %collective-permute-start.1 = (bf16[128,1]{0,1:T(2,128)(2,1)S(1)}, bf16[128,1]{0,1:T(2,128)(2,1)S(1)}, u32[]{:S(2)}, u32[]{:S(2)}) collective-permute-start(bf16[128,1]{0,1:T(2,128)(2,1)S(1)} %get-tuple-element.43), channel_id=1, source_target_pairs={{0,2},{2,4},{4,6},{6,8},{8,10},{10,12},{12,14},{1,3},{3,5},{5,7},{... | collective-permute-start | bytes 776 | tf_op jit(solution)/shard_map/ppermute | solution.py:25
  16.9 78.3 %copy-start.4 = (bf16[256,128]{1,0:T(8,128)(2,1)S(1)}, bf16[256,128]{1,0:T(8,128)(2,1)}, u32[]{:S(2)}) copy-start(bf16[256,128]{1,0:T(8,128)(2,1)} %param.17) | copy-start | bytes 196612
  16.9 96.3 %copy-start.8 = (f32[8]{0:T(128)S(1)}, f32[8]{0:T(128)}, u32[]{:S(2)}) copy-start(f32[8]{0:T(128)} %param.24) | copy-start | bytes 100
  16.9 142.3 %all-to-all-start = ((bf16[8,256,512]{2,1,0:T(8,128)(2,1)}), bf16[8,256,512]{2,1,0:T(8,128)(2,1)}, u32[]{:S(2)}, u32[]{:S(2)}) async-start(bf16[8,256,512]{2,1,0:T(8,128)(2,1)} %stack.2), calls=%async_computation | async-start | bytes 4194304 | tf_op jit(solution)/shard_map/all_to_all | solution.py:14
  23.4 93.5 %copy-start.6 = (f32[2048]{0:T(1024)S(1)}, f32[2048]{0:T(1024)}, u32[]{:S(2)}) copy-start(f32[2048]{0:T(1024)} %param.15) | copy-start | bytes 24580
  23.4 164.2 %all-gather.15.cloned.1.call-start = ((), (), s32[]{:S(2)}) async-start(), calls=%async_computation.4 | async-start | bytes 2359296 | tf_op jit(solution)/shard_map/all_gather | solution.py:91
  24.0 191.6 %all-gather.13.cloned.1.call-start = ((), (), s32[]{:S(2)}) async-start(), calls=%async_computation.3 | async-start | bytes 2359296 | tf_op jit(solution)/shard_map/all_gather | solution.py:154
  114.2 2.9 %copy-start = (bf16[768,2048]{1,0:T(8,128)(2,1)S(1)}, bf16[768,2048]{1,0:T(8,128)(2,1)}, u32[]{:S(2)}) copy-start(bf16[768,2048]{1,0:T(8,128)(2,1)} %all-gather.9.cloned.1.call-done) | copy-start | bytes 9437188
  119.6 4.5 %collective-permute-start = (bf16[128,256]{0,1:T(8,128)(2,1)S(1)}, bf16[128,256]{0,1:T(8,128)(2,1)S(1)}, u32[]{:S(2)}, u32[]{:S(2)}) collective-permute-start(bf16[128,256]{0,1:T(8,128)(2,1)S(1)} %get-tuple-element.24), channel_id=1, source_target_pairs={{0,2},{2,4},{4,6},{6,8},{8,10},{10,12},{12,14},{1,3},{3,5},{5,7},{... | collective-permute-start | bytes 196616 | tf_op jit(solution)/shard_map/ppermute | solution.py:25
  121.9 4.0 %collective-permute-start.3 = (bf16[128,256]{0,1:T(8,128)(2,1)S(1)}, bf16[128,256]{0,1:T(8,128)(2,1)S(1)}, u32[]{:S(2)}, u32[]{:S(2)}) collective-permute-start(bf16[128,256]{0,1:T(8,128)(2,1)S(1)} %get-tuple-element.25), channel_id=1, source_target_pairs={{2,0},{4,2},{6,4},{8,6},{10,8},{12,10},{14,12},{3,1},{5,3},{7,5},{... | collective-permute-start | bytes 196616 | tf_op jit(solution)/shard_map/ppermute | solution.py:27
  139.5 12.2 %copy-start.5 = (f32[3,512]{1,0:T(4,128)S(1)}, f32[3,512]{1,0:T(4,128)}, u32[]{:S(2)}) copy-start(f32[3,512]{1,0:T(4,128)} %param.25) | copy-start | bytes 18436
  143.0 103.4 %all-gather.23.cloned.1.call-start = ((), (), s32[]{:S(2)}) async-start(), calls=%async_computation.8 | async-start | bytes 2359296 | tf_op jit(solution)/shard_map/all_gather | solution.py:92
  143.8 130.8 %all-gather.21.cloned.1.call-start = ((), (), s32[]{:S(2)}) async-start(), calls=%async_computation.7 | async-start | bytes 2359296 | tf_op jit(solution)/shard_map/all_gather | solution.py:157
  144.4 7.3 %collective-permute-start.5 = (bf16[1,1]{0,1:T(2,128)(2,1)}, bf16[1,1]{0,1:T(2,128)(2,1)}, u32[]{:S(2)}, u32[]{:S(2)}) collective-permute-start(bf16[1,1]{0,1:T(2,128)(2,1)} %bitcast.27), channel_id=1, source_target_pairs={{2,0},{4,2},{6,4},{8,6},{10,8},{12,10},{14,12},{3,1},{5,3},{7,5},{... | collective-permute-start | bytes 14 | tf_op jit(solution)/shard_map/ppermute | solution.py:27
  145.7 6.5 %collective-permute-start.4 = (bf16[1,1]{0,1:T(2,128)(2,1)}, bf16[1,1]{0,1:T(2,128)(2,1)}, u32[]{:S(2)}, u32[]{:S(2)}) collective-permute-start(bf16[1,1]{0,1:T(2,128)(2,1)} %bitcast.26), channel_id=1, source_target_pairs={{0,2},{2,4},{4,6},{6,8},{8,10},{10,12},{12,14},{1,3},{3,5},{5,7},{... | collective-permute-start | bytes 14 | tf_op jit(solution)/shard_map/ppermute | solution.py:25
  153.6 5.7 %copy-start.1 = (bf16[768,2048]{1,0:T(8,128)(2,1)S(1)}, bf16[768,2048]{1,0:T(8,128)(2,1)}, u32[]{:S(2)}) copy-start(bf16[768,2048]{1,0:T(8,128)(2,1)} %all-gather.9.cloned.1.call-done) | copy-start | bytes 9437188
  159.3 10.5 %copy-start.7 = (f32[512]{0:T(512)S(1)}, f32[512]{0:T(512)}, u32[]{:S(2)}) copy-start(f32[512]{0:T(512)} %param.26) | copy-start | bytes 6148
  163.2 6.1 %copy-start.2 = (bf16[768,512]{0,1:T(8,128)(2,1)}, bf16[768,512]{0,1:T(8,128)(2,1)S(1)}, u32[]{:S(2)}) copy-start(bf16[768,512]{0,1:T(8,128)(2,1)S(1)} %multiply_convert_fusion.1) | copy-start | bytes 2359300
  163.3 6.1 %collective-permute-start.7 = (bf16[1,512]{0,1:T(8,128)(2,1)S(1)}, bf16[1,512]{0,1:T(8,128)(2,1)}, u32[]{:S(2)}, u32[]{:S(2)}) collective-permute-start(bf16[1,512]{0,1:T(8,128)(2,1)S(1)} %get-tuple-element.13), channel_id=1, source_target_pairs={{2,0},{4,2},{6,4},{8,6},{10,8},{12,10},{14,12},{3,1},{5,3},{7,5},{... | collective-permute-start | bytes 3080 | tf_op jit(solution)/shard_map/ppermute | solution.py:27
  164.6 5.1 %collective-permute-start.6 = (bf16[1,512]{0,1:T(8,128)(2,1)S(1)}, bf16[1,512]{0,1:T(8,128)(2,1)}, u32[]{:S(2)}, u32[]{:S(2)}) collective-permute-start(bf16[1,512]{0,1:T(8,128)(2,1)S(1)} %get-tuple-element.12), channel_id=1, source_target_pairs={{0,2},{2,4},{4,6},{6,8},{8,10},{10,12},{12,14},{1,3},{3,5},{5,7},{... | collective-permute-start | bytes 3080 | tf_op jit(solution)/shard_map/ppermute | solution.py:25
Sparse Core Ops, SparseCore 0:
  8.9 47.6 all-gather.8
  58.1 36.6 all-gather.10
  96.4 29.5 all-gather.18
  127.4 28.7 all-gather.16
  157.6 29.9 all-gather.14
  189.0 26.5 all-gather.12
  217.2 29.1 all-gather.22
  248.0 26.5 all-gather.20
